TPU v7x, 32 devices: a whole 2x2x4 slice. The times are simulated.
32 devices in a mesh: sp: 8 (over z, y), tp: 4 (over x, core).
Axes of the slice: x: 2, y: 2, z: 4, core: 2. Of those that a mesh axis runs over, the one named last changes fastest.
Arguments:
- memory_queries: bfloat16 [4096, 1024], P('sp', 'tp'), may hold values from -8 to 8
- memory_keys: bfloat16 [4096, 1024], P('sp', 'tp'), may hold values from -8 to 8
- memory_values: bfloat16 [4096, 1024], P('sp', 'tp'), may hold values from -6 to 6
- input_gate_logits: float32 [8, 4096], P('tp', 'sp'), may hold values from -64 to 160
- forget_gate_logits: float32 [8, 4096], P('tp', 'sp'), may hold values from -0.1 to 20
- extra_log_decay: float32 [8, 4096], P('tp', 'sp'), may hold values from -1.4 to 0
- residual: bfloat16 [4096, 2048], P(('sp', 'tp')), may hold values from -6 to 6
- cell_output_weight: bfloat16 [1024, 2048], P('tp', 'sp'), may hold values from -0.1875 to 0.1875
- expert_norm_gain: float32 [2048], replicated, may hold values from 0.1 to 1.9
- expert_gate_weight: bfloat16 [8, 2048, 3584], P('sp', None, 'tp'), may hold values from -0.125 to 0.125
- expert_up_weight: bfloat16 [8, 2048, 3584], P('sp', None, 'tp'), may hold values from -0.125 to 0.125
- expert_down_weight: bfloat16 [8, 3584, 2048], P('sp', 'tp'), may hold values from -0.09375 to 0.09375
- routed_expert_index: int32 [4096, 2], P('sp'), may hold values from 0 to 7, as said below
- routed_expert_weight: float32 [4096, 2], P(('sp', 'tp')), may hold values from 0.1 to 1
Outputs:
- layer_out: bfloat16 [4096, 2048], P(('sp', 'tp'))
Inputs may be any that keep to these rules, and one draw needn't show every extreme that they name: `routed_expert_index`: each row names 2 different experts. In each aligned block of 128 rows (the rows of one device after the cell) no expert is named more than 40 times, and one expert is named exactly 40 times in every block.
All inputs are finite; a program needn't handle non-finite values.
Results may differ from a plain program's by a relative error of at most 0.013.
Values may be sent and summed in bfloat16 or wider, within the bound.
A program may use at most 128 MiB of HBM per device.

v0:
```python
import jax
import jax.numpy as jnp
from jax import lax
from jax.sharding import PartitionSpec as P

highest = lax.Precision.HIGHEST
lowest = -1e30
epsilon = 1e-06


def carried_in(x, axis, combine, identity):
    length, place = (lax.axis_size(axis), lax.axis_index(axis))
    everything = jax.tree.map(lambda part: lax.all_gather(part, axis), x)
    start = jax.tree.map(
        lambda part, zero: jnp.broadcast_to(jnp.asarray(zero, part.dtype), part.shape), x, identity
    )

    def turn(k, before):
        reached = k < place
        new = combine(before, jax.tree.map(lambda part: part[k], everything))
        return jax.tree.map(lambda a, b: jnp.where(reached, a, b), new, before)

    return lax.fori_loop(0, length, turn, start)


def block_pass(memory, inputs):
    state_mat, state_norm, state_max = memory
    queries, keys_blk, values_blk, gate_in, forget_log_value = inputs
    length = gate_in.shape[-1]
    running = jnp.cumsum(forget_log_value, axis=-1)
    causal = jnp.arange(length)[:, None] >= jnp.arange(length)[None, :]
    exponent = running[:, :, None] - running[:, None, :] + gate_in[:, None, :]
    exponent = jnp.where(causal[None], exponent, -jnp.inf)
    carried = running + state_max[:, None]
    row_max = jnp.maximum(carried, jnp.max(exponent, axis=-1))
    decays = jnp.exp(exponent - row_max[:, :, None])
    carry_scale = jnp.exp(carried - row_max)
    dispatch_affinity = jnp.einsum("htk,hsk->hts", queries, keys_blk, precision=highest) * decays
    numerator = carry_scale[:, :, None] * jnp.einsum(
        "hvk,htk->htv", state_mat, queries, precision=highest
    )
    numerator = numerator + jnp.einsum(
        "hts,hsv->htv", dispatch_affinity, values_blk, precision=highest
    )
    denominator = carry_scale * jnp.einsum(
        "hk,htk->ht", state_norm, queries, precision=highest
    ) + jnp.sum(dispatch_affinity, axis=-1)
    final_log = running[:, -1]
    log_prev = final_log + state_max
    log_keep = final_log[:, None] - running + gate_in
    new_max = jnp.maximum(log_prev, jnp.max(log_keep, axis=-1))
    prev_scale = jnp.exp(log_prev - new_max)
    retain = jnp.exp(log_keep - new_max[:, None])
    new_mat = prev_scale[:, None, None] * state_mat + jnp.einsum(
        "hsv,hsk->hvk", retain[:, :, None] * values_blk, keys_blk, precision=highest
    )
    new_norm = prev_scale[:, None] * state_norm + jnp.einsum(
        "hs,hsk->hk", retain, keys_blk, precision=highest
    )
    return ((new_mat, new_norm, new_max), (numerator, denominator, row_max))


def join_states(earlier, later):
    early_log, early_mat, early_norm, early_max = earlier
    late_log, late_mat, late_norm, late_max = later
    joined_max = jnp.maximum(early_max + late_log, late_max)
    early_scale = jnp.exp(early_max + late_log - joined_max)
    late_scale = jnp.exp(late_max - joined_max)
    joined_mat = early_scale[:, None, None] * early_mat + late_scale[:, None, None] * late_mat
    joined_norm = early_scale[:, None] * early_norm + late_scale[:, None] * late_norm
    return (early_log + late_log, joined_mat, joined_norm, joined_max)


def matrix_memory_step(
    memory_queries,
    memory_keys,
    memory_values,
    input_gate_logits,
    forget_gate_logits,
    extra_log_decay,
):
    tokens_here, channels = memory_queries.shape
    heads_here = input_gate_logits.shape[0]
    head_dim = channels // heads_here

    def heads_first(tensor):
        return jnp.transpose(
            tensor.astype(jnp.float32).reshape(tokens_here, heads_here, head_dim), (1, 0, 2)
        )

    queries = heads_first(memory_queries) * head_dim ** (-0.5)
    forget_log_value = jax.nn.log_sigmoid(forget_gate_logits) + extra_log_decay
    block_size = min(tokens_here, 256)
    block_count = tokens_here // block_size

    def split_blocks(tensor):
        return jnp.moveaxis(
            tensor.reshape((heads_here, block_count, block_size) + tensor.shape[2:]), 1, 0
        )

    def join_blocks(tensor):
        return jnp.moveaxis(tensor, 0, 1).reshape((heads_here, tokens_here) + tensor.shape[3:])

    empty_state = (
        jnp.zeros((heads_here, head_dim, head_dim), jnp.float32),
        jnp.zeros((heads_here, head_dim), jnp.float32),
        jnp.full((heads_here,), lowest, jnp.float32),
    )
    members = (
        queries,
        heads_first(memory_keys),
        heads_first(memory_values),
        input_gate_logits,
        forget_log_value,
    )
    end_state, pieces = lax.scan(
        block_pass, empty_state, tuple((split_blocks(member) for member in members))
    )
    numerator, denominator, row_max = (join_blocks(member) for member in pieces)
    running = jnp.cumsum(forget_log_value, axis=-1)
    identity = (jnp.zeros((heads_here,), jnp.float32),) + empty_state
    incoming = carried_in((running[:, -1],) + tuple(end_state), "sp", join_states, identity)
    prior_mat, prior_norm, prior_max = incoming[1:]
    reached = running + prior_max[:, None]
    joined = jnp.maximum(row_max, reached)
    local_scale = jnp.exp(row_max - joined)
    carry_scale = jnp.exp(reached - joined)
    numerator = local_scale[:, :, None] * numerator + carry_scale[:, :, None] * jnp.einsum(
        "hvk,htk->htv", prior_mat, queries, precision=highest
    )
    denominator = local_scale * denominator + carry_scale * jnp.einsum(
        "hk,htk->ht", prior_norm, queries, precision=highest
    )
    guarded = jnp.maximum(jnp.abs(denominator), jnp.exp(-joined))
    return ((numerator / guarded[:, :, None]).astype(jnp.bfloat16), heads_here, head_dim)


def slot_index(ids, experts, capacity):
    flat_ids = ids.reshape(-1)
    matches = (flat_ids[:, None] == jnp.arange(experts, dtype=jnp.int32)[None, :]).astype(jnp.int32)
    before = jnp.cumsum(matches, axis=0) - matches
    return flat_ids * capacity + jnp.sum(before * matches, axis=1)


def local(
    memory_queries,
    memory_keys,
    memory_values,
    input_gate_logits,
    forget_gate_logits,
    extra_log_decay,
    residual,
    cell_output_weight,
    expert_norm_gain,
    expert_gate_weight,
    expert_up_weight,
    expert_down_weight,
    routed_expert_index,
    routed_expert_weight,
):
    hidden, heads_here, head_dim = matrix_memory_step(
        memory_queries,
        memory_keys,
        memory_values,
        input_gate_logits,
        forget_gate_logits,
        extra_log_decay,
    )
    weight_piece = lax.all_gather(cell_output_weight, "sp", axis=1, tiled=True)
    shaped = weight_piece.reshape(heads_here, head_dim, weight_piece.shape[1])
    partial_rows = jnp.einsum(
        "htd,hdc->tc", hidden, shaped, preferred_element_type=jnp.float32
    ).astype(jnp.bfloat16)
    projected = lax.psum_scatter(
        partial_rows.astype(jnp.float32).astype(jnp.bfloat16), "tp", scatter_dimension=0, tiled=True
    ).astype(jnp.float32)
    mixed_rows = (residual.astype(jnp.float32) + projected).astype(jnp.bfloat16)
    mixed_wide = mixed_rows.astype(jnp.float32)
    norm_scale = lax.rsqrt(jnp.mean(mixed_wide * mixed_wide, axis=-1, keepdims=True) + epsilon)
    normed = (mixed_wide * norm_scale * expert_norm_gain).astype(jnp.bfloat16)
    sp_size = lax.axis_size("sp")
    row_count, model_width = residual.shape
    top_count = routed_expert_index.shape[1]
    experts = sp_size * expert_gate_weight.shape[0]
    assigned = row_count * top_count
    capacity = max(2, assigned * 5 // (4 * experts))
    own_ids = lax.dynamic_slice_in_dim(
        routed_expert_index, lax.axis_index("tp") * row_count, row_count, 0
    )
    own_slots = slot_index(own_ids, experts, capacity)
    zero_row = jnp.zeros((1, model_width), jnp.bfloat16)
    padded = jnp.concatenate([normed, zero_row], axis=0)
    slot_table = jnp.full((experts * capacity,), row_count, jnp.int32)
    slot_table = slot_table.at[own_slots].set(jnp.arange(assigned, dtype=jnp.int32) // top_count)
    arrived = lax.all_gather(
        lax.all_to_all(
            padded[slot_table.reshape(experts, 1, capacity)],
            "sp",
            split_axis=0,
            concat_axis=0,
            tiled=True,
        ),
        "tp",
        axis=1,
        tiled=True,
    )
    sources, owners, slot_span, width_in = arrived.shape
    flat_rows = arrived.reshape(-1, width_in)
    gate_pre = jnp.dot(flat_rows, expert_gate_weight[0], preferred_element_type=jnp.float32)
    up_pre = jnp.dot(flat_rows, expert_up_weight[0], preferred_element_type=jnp.float32)
    hidden_act = (jax.nn.silu(gate_pre) * up_pre).astype(jnp.bfloat16)
    group_term = jnp.dot(hidden_act, expert_down_weight[0], preferred_element_type=jnp.float32)
    group_term = lax.optimization_barrier(group_term.astype(jnp.bfloat16)).astype(jnp.float32)
    summed = lax.psum_scatter(
        group_term.reshape(sources, owners, slot_span, width_in).astype(jnp.bfloat16),
        "tp",
        scatter_dimension=1,
        tiled=True,
    )
    returned = lax.all_to_all(summed, "sp", split_axis=0, concat_axis=0, tiled=True)
    picked = returned.reshape(experts * capacity, model_width)[own_slots]
    picked = picked.reshape(row_count, top_count, model_width).astype(jnp.float32)
    routed_sum = jnp.sum(picked * routed_expert_weight[:, :, None], axis=1)
    return (mixed_wide + routed_sum).astype(jnp.bfloat16)


def solution(mesh):
    return jax.shard_map(
        local,
        mesh=mesh,
        in_specs=(
            P("sp", "tp"),
            P("sp", "tp"),
            P("sp", "tp"),
            P("tp", "sp"),
            P("tp", "sp"),
            P("tp", "sp"),
            P(("sp", "tp"), None),
            P("tp", "sp"),
            P(),
            P("sp", None, "tp"),
            P("sp", None, "tp"),
            P("sp", "tp", None),
            P("sp", None),
            P(("sp", "tp"), None),
        ),
        out_specs=P(("sp", "tp"), None),
        check_vma=False,
    )
```

profile of v0, /device:TPU:0, one launch (start us, length us, event | category | flops | bytes accessed | tf_op | source)
XLA Modules:
  0.0 404.9 jit_solution(8255470432722626242)
XLA Ops:
  6.6 1.1 copy.56
  8.0 1.1 copy.54
  9.9 11.3 %while.39 = (s32[]{:T(128)}, f32[2,128,128]{2,1,0:T(8,128)S(1)}, f32[2,128]{1,0:T(2,128)S(1)}, f32[2]{0:T(128)S(1)}, f32[2,2,256,128]{3,2,0,1:T(8,128)S(1)}, /*i...) while((s32[]{:T(128)}, f32[2,128,128]{2,1,0:T(8,128)S(1)}, ...), condition=%wide.region_6.7_spmd.clone, body=%wide.region_0.6_spmd.clone.sunk | while | flops 607329536 | bytes 4625314 | solution.py:116
  9.9 0.6 reduce-window.38
  11.7 0.6 fusion.123
  13.6 1.0 fusion.125
  14.8 0.7 convolution_add_fusion.3
  15.6 0.6 reduce-window.38
  17.3 0.6 fusion.123
  19.3 1.0 fusion.125
  20.4 0.7 convolution_add_fusion.3
  21.2 0.6 copy-done
  21.9 0.7 all-gather.9.cloned.1.call-update
  22.7 0.6 reduce-window.22
  23.9 0.7 dynamic-slice
  25.6 23.2 %all-reduce.4 = (f32[16]{0:T(128)S(1)}, f32[16]{0:T(128)S(1)}) all-reduce(f32[16]{0:T(128)S(1)} %bitcast_dynamic-update-slice_fusion.1, f32[16]{0:T(128)S(1)} %dynamic-update-slice.1), channel_id=2, replica_groups=mesh['sp'=8,'tp'=4] {'sp'}, use_global_device_ids=true, to_apply=%add.1 | all-reduce | flops 32 | bytes 256
  49.0 16.4 %all-gather.4 = f32[8,2,128]{2,1,0:T(2,128)S(1)} all-gather(f32[1,2,128]{2,1,0:T(2,128)S(1)} %bitcast.293), channel_id=5, replica_groups=mesh['sp'=8,'tp'=4] {'sp'}, dimensions={0}, use_global_device_ids=true | all-gather | bytes 9216 | tf_op jit(solution)/shard_map/all_gather | solution.py:13
  65.4 9.0 %while.40 = (s32[]{:T(128)}, f32[2,128,128]{2,1,0:T(8,128)S(1)}, f32[2,128]{1,0:T(2,128)S(1)}, f32[2]{0:T(128)S(1)}, s32[]{:T(128)}, /*index=5*/f32[8,2]{1,0:T(8...) while((s32[]{:T(128)}, f32[2,128,128]{2,1,0:T(8,128)S(1)}, ...), condition=%wide.region_10.11_spmd.clone, body=%wide.region_9.10_spmd.clone.sunk | while | flops 165138 | bytes 396541 | solution.py:23
  65.5 1.0 fusion.126
  66.6 1.0 fusion.126
  67.7 1.0 fusion.126
  68.8 1.0 fusion.126
  69.9 1.0 fusion.126
  71.1 1.0 fusion.126
  72.2 1.0 fusion.126
  73.3 1.0 fusion.126
  75.1 1.2 fusion.47
  76.3 29.1 %all-gather.9.cloned.1.call-done = bf16[256,2048]{1,0:T(8,128)(2,1)} async-done(((bf16[256,256]{1,0:T(8,128)(2,1)}), bf16[256,2048]{1,0:T(8,128)(2,1)}) %all-gather.9.cloned.1.call-update) | async-done | bytes 1048592 | tf_op jit(solution)/shard_map/all_gather | solution.py:169
  105.3 3.3 bitcast_convert_fusion
  108.7 0.7 broadcast_multiply_fusion
  111.0 1.4 scatter_custom_fusion
  112.6 26.4 %reduce-scatter.3.cloned.1.call-done = bf16[128,2048]{1,0:T(8,128)(2,1)} async-done(((bf16[512,2048]{1,0:T(8,128)(2,1)}), bf16[128,2048]{1,0:T(8,128)(2,1)}) %reduce-scatter.3.cloned.1.call-update) | async-done | bytes 524304 | tf_op jit(solution)/shard_map/reduce_scatter | solution.py:174
  139.0 1.3 fusion.48
  140.3 1.3 fusion.50
  141.6 2.4 gather_fusion
  144.0 36.6 %all_to_all.10 = bf16[8,1,40,2048]{3,2,1,0:T(8,128)(2,1)} all-to-all(bf16[8,1,40,2048]{3,2,1,0:T(8,128)(2,1)S(1)} %bitcast.275), channel_id=1, replica_groups=mesh['sp'=8,'tp'=4] {'sp'}, dimensions={0} | all-to-all | bytes 2621440 | tf_op jit(solution)/shard_map/all_to_all | solution.py:196
  180.9 38.4 %all-gather.11.cloned.1.call-done = bf16[8,4,40,2048]{3,2,1,0:T(8,128)(2,1)} async-done(((bf16[8,1,40,2048]{3,2,1,0:T(8,128)(2,1)}), bf16[8,4,40,2048]{3,2,1,0:T(8,128)(2,1)}) %all-gather.11.cloned.1.call-update) | async-done | bytes 5242896 | tf_op jit(solution)/shard_map/all_gather | solution.py:195
  219.3 10.0 %fusion.43 = f32[1280,896]{1,0:T(8,128)} fusion(bf16[1280,2048]{1,0:T(8,128)(2,1)} %bitcast.302, bf16[1,2048,896]{2,1,0:T(8,128)(2,1)} %param.27), kind=kOutput, calls=%fused_computation.81 | convolution fusion | flops 4697620480 | bytes 13500416 | tf_op jit(solution)/shard_map/dot_general | solution.py:209
  229.3 17.6 %convolution_convert_fusion = bf16[1280,2048]{1,0:T(8,128)(2,1)} fusion(bf16[1,896,2048]{2,1,0:T(8,128)(2,1)} %param.29, f32[1280,896]{1,0:T(8,128)} %fusion.43, bf16[1280,2048]{1,0:T(8,128)(2,1)} %bitcast.303, bf16[1,2048,896]{2,1,0:T(8,128)(2,1)} %param.28), kind=kOutput, calls=%fused_computation.76 | convolution fusion | flops 9404743680 | bytes 22413312 | tf_op jit(solution)/shard_map/dot_general | solution.py:212
  246.9 0.6 copy-done.9
  248.1 101.5 %all-reduce.7.cloned.1.call-done = bf16[8,4,40,2048]{3,2,1,0:T(8,128)(2,1)} async-done(((bf16[8,4,40,2048]{3,2,1,0:T(8,128)(2,1)}), bf16[8,4,40,2048]{3,2,1,0:T(8,128)(2,1)}) %all-reduce.7.cloned.1.call-update) | async-done | bytes 5242896
  349.6 3.2 constant_dynamic-slice_fusion.3
  352.8 5.5 %all-to-all-start.1 = ((bf16[8,1,40,2048]{3,2,1,0:T(8,128)(2,1)}), bf16[8,1,40,2048]{3,2,1,0:T(8,128)(2,1)S(1)}, u32[]{:S(2)}, u32[]{:S(2)}) async-start(bf16[8,1,40,2048]{3,2,1,0:T(8,128)(2,1)} %constant_dynamic-slice_fusion.3), calls=%async_computation.2 | async-start | bytes 2621440 | tf_op jit(solution)/shard_map/all_to_all | solution.py:220
  358.5 30.9 %all-to-all-done.1 = bf16[8,1,40,2048]{3,2,1,0:T(8,128)(2,1)S(1)} async-done(((bf16[8,1,40,2048]{3,2,1,0:T(8,128)(2,1)}), bf16[8,1,40,2048]{3,2,1,0:T(8,128)(2,1)S(1)}, u32[]{:S(2)}, u32[]{:S(2)}) %all-to-all-start.1) | async-done | bytes 1310752 | tf_op jit(solution)/shard_map/all_to_all | solution.py:220
  389.4 2.3 gather_fusion.1
  391.7 2.4 reshape.428
  394.2 3.2 multiply_reduce_fusion
  397.3 1.0 fusion.51
  (153 shorter events, 11.6 us)
Async XLA Ops:
  6.5 2.9 copy-start.3
  6.5 3.3 copy-start.7
  6.5 3.3 copy-start.6
  6.5 3.3 copy-start.4
  6.5 58.9 %all-gather.13.cloned.1.call-start = ((), (), s32[]{:S(2)}) async-start(), calls=%async_computation.6 | async-start | bytes 1179648 | tf_op jit(solution)/shard_map/all_gather | solution.py:13
  9.9 14.0 %copy-start.10 = (u32[32]{0:T(128)S(1)}, u32[32]{0:T(128)}, u32[]{:S(2)}) copy-start(u32[32]{0:T(128)} %constant.125) | copy-start | bytes 388
  21.2 0.7 copy-start
  21.8 83.5 %all-gather.9.cloned.1.call-start = ((), (), s32[]{:S(2)}) async-start(), calls=%async_computation.3 | async-start | bytes 1179648 | tf_op jit(solution)/shard_map/all_gather | solution.py:169
  22.6 116.4 %reduce-scatter.3.cloned.1.call-start = ((), (), s32[]{:S(2)}) async-start(), calls=%async_computation.4 | async-start | bytes 2621440 | tf_op jit(solution)/shard_map/reduce_scatter | solution.py:174
  75.1 63.9 %copy-start.1 = (bf16[128,2048]{1,0:T(8,128)(2,1)S(1)}, bf16[128,2048]{1,0:T(8,128)(2,1)}, u32[]{:S(2)}) copy-start(bf16[128,2048]{1,0:T(8,128)(2,1)} %param.24) | copy-start | bytes 1572868
  76.2 64.0 %copy-start.5 = (f32[2048]{0:T(1024)S(1)}, f32[2048]{0:T(1024)}, u32[]{:S(2)}) copy-start(f32[2048]{0:T(1024)} %param.26) | copy-start | bytes 24580
  108.6 110.7 %all-gather.11.cloned.1.call-start = ((), (), s32[]{:S(2)}) async-start(), calls=%async_computation.5 | async-start | bytes 6553600 | tf_op jit(solution)/shard_map/all_gather | solution.py:195
  180.7 168.9 %all-reduce.7.cloned.1.call-start = ((), (), s32[]{:S(2)}) async-start(), calls=%async_computation.7 | async-start | bytes 10485760
  246.9 0.7 copy-start.9
  246.9 111.4 %copy-start.8 = (f32[128,2]{0,1:T(2,128)S(1)}, f32[128,2]{0,1:T(2,128)}, u32[]{:S(2)}) copy-start(f32[128,2]{0,1:T(2,128)} %param.31) | copy-start | bytes 3076
  352.8 36.5 %all-to-all-start.1 = ((bf16[8,1,40,2048]{3,2,1,0:T(8,128)(2,1)}), bf16[8,1,40,2048]{3,2,1,0:T(8,128)(2,1)S(1)}, u32[]{:S(2)}, u32[]{:S(2)}) async-start(bf16[8,1,40,2048]{3,2,1,0:T(8,128)(2,1)} %constant_dynamic-slice_fusion.3), calls=%async_computation.2 | async-start | bytes 2621440 | tf_op jit(solution)/shard_map/all_to_all | solution.py:220
  391.7 5.6 %copy-start.2 = (bf16[128,2048]{1,0:T(8,128)(2,1)S(1)}, bf16[128,2048]{1,0:T(8,128)(2,1)}, u32[]{:S(2)}) copy-start(bf16[128,2048]{1,0:T(8,128)(2,1)} %reduce-scatter.3.cloned.1.call-done) | copy-start | bytes 1572868
Sparse Core Ops, SparseCore 0:
  22.0 43.1 all-gather.12
  67.2 38.0 all-gather.8
  108.8 30.1 reduce-scatter.2
  180.8 38.4 all-gather.10
  247.0 102.5 all-reduce.6
where the time goes:
time: 406 us; the launch traced here: 405 us
  waiting for transfers between devices  227 us (56%)
  blocking collectives  76.3 us (19%)
  matrix products  39.1 us (10%)
  other arithmetic  22 us (5%)
  local copies, waits for them, and re-layouts  20.1 us (5%)
  between operations  14.2 us (3%)
  starting transfers between devices  5.89 us (1%)
    unnamed x6, waiting for transfers between devices  102 us
    all_gather x1, waiting for transfers between devices, local(): lax.all_gather(lax.all_to_all(padded[slot_table.reshape(experts, 1, capac...  38.4 us
    all_to_all x1, blocking collectives, local(): lax.all_to_all(padded[slot_table.reshape(experts, 1, capacity)], 'sp', sp...  36.6 us
    all_to_all x1, waiting for transfers between devices, local(): lax.all_to_all(summed, 'sp', split_axis=0, concat_axis=0, tiled=True)  30.9 us
    all_gather x1, waiting for transfers between devices, local(): weight_piece = lax.all_gather(cell_output_weight, 'sp', axis=1, tiled=True)  29.1 us
    reduce_scatter x1, waiting for transfers between devices, local(): lax.psum_scatter(partial_rows.astype(jnp.float32).astype(jnp.bfloat16), '...  26.4 us
    unnamed x1, blocking collectives  23.2 us
    dot_general x1, matrix products, local(): jnp.dot(hidden_act, expert_down_weight[0], preferred_element_type=jnp.flo...  17.6 us
  transfers between devices with their start and end apart: 6, of which 5 were waited for; matrix products, arithmetic and copies ran while one was open for 4% of the time, Pallas kernels for 0%

commit v1 on v0

--- a/solution.py
+++ b/solution.py
@@ -166,7 +166,12 @@
         forget_gate_logits,
         extra_log_decay,
     )
-    weight_piece = lax.all_gather(cell_output_weight, "sp", axis=1, tiled=True)
+    ring = [cell_output_weight]
+    for hop in range(7):
+        ring.append(lax.ppermute(ring[-1], "sp", [(dev, (dev + 1) % 8) for dev in range(8)]))
+    weight_piece = jnp.roll(
+        jnp.concatenate(ring[::-1], axis=1), (lax.axis_index("sp") + 1) * ring[0].shape[1], axis=1
+    )
     shaped = weight_piece.reshape(heads_here, head_dim, weight_piece.shape[1])
     partial_rows = jnp.einsum(
         "htd,hdc->tc", hidden, shaped, preferred_element_type=jnp.float32

time: 406 us -> 416 us (1.025)
  local copies, waits for them, and re-layouts: 20.1 us -> 26.2 us
    ppermute x0 -> x7, waiting for transfers between devices: none -> 34.3 us  [local(): lax.ppermute(ring[-1], 'sp', [(dev, (dev + 1) % 8) for dev in range(8)])]
    all_gather x1 -> x0, waiting for transfers between devices: 29.1 us -> none  [local(): weight_piece = lax.all_gather(cell_output_weight, 'sp', axis=1, tiled=True)]
    unnamed x35 -> x54, local copies, waits for them, and re-layouts: 8.66 us -> 14.5 us
    unnamed x6 -> x5, waiting for transfers between devices: 102 us -> 102 us
  transfers between devices with their start and end apart: 6 -> 12, of which waited for: 5 -> 9; matrix products, arithmetic and copies ran while one was open for 4% -> 7% of each run, Pallas kernels for 0% -> 0%
where the time goes in v1:
time: 416 us; the launch traced here: 415 us
  waiting for transfers between devices  231 us (56%)
  blocking collectives  74.9 us (18%)
  matrix products  38 us (9%)
  local copies, waits for them, and re-layouts  26.2 us (6%)
  other arithmetic  22 us (5%)
  between operations  14.3 us (3%)
  starting transfers between devices  8.66 us (2%)
    unnamed x5, waiting for transfers between devices  102 us
    all_gather x1, waiting for transfers between devices, local(): lax.all_gather(lax.all_to_all(padded[slot_table.reshape(experts, 1, capac...  38.6 us
    all_to_all x1, blocking collectives, local(): lax.all_to_all(padded[slot_table.reshape(experts, 1, capacity)], 'sp', sp...  36.6 us
    ppermute x7, waiting for transfers between devices, local(): lax.ppermute(ring[-1], 'sp', [(dev, (dev + 1) % 8) for dev in range(8)])  34.3 us
    all_to_all x1, waiting for transfers between devices, local(): lax.all_to_all(summed, 'sp', split_axis=0, concat_axis=0, tiled=True)  30.9 us
    reduce_scatter x1, waiting for transfers between devices, local(): lax.psum_scatter(partial_rows.astype(jnp.float32).astype(jnp.bfloat16), '...  25.9 us
    unnamed x1, blocking collectives  21.9 us
    dot_general x1, matrix products, local(): jnp.dot(hidden_act, expert_down_weight[0], preferred_element_type=jnp.flo...  17.6 us
  transfers between devices with their start and end apart: 12, of which 9 were waited for; matrix products, arithmetic and copies ran while one was open for 7% of the time, Pallas kernels for 0%

profile of v1, /device:TPU:0, one launch (start us, length us, event | category | flops | bytes accessed | tf_op | source)
XLA Modules:
  0.0 415.5 jit_solution(683908669876277390)
XLA Ops:
  6.5 3.0 collective-permute-start
  9.5 1.1 copy.56
  11.1 5.2 %collective-permute-done = bf16[256,256]{1,0:T(8,128)(2,1)S(1)} collective-permute-done((bf16[256,256]{1,0:T(8,128)(2,1)}, bf16[256,256]{1,0:T(8,128)(2,1)S(1)}, u32[]{:S(2)}, u32[]{:S(2)}) %collective-permute-start) | collective-permute-done | bytes 131104 | tf_op jit(solution)/shard_map/ppermute | solution.py:171
  16.7 7.3 %collective-permute-done.1 = bf16[256,256]{1,0:T(8,128)(2,1)} collective-permute-done((bf16[256,256]{1,0:T(8,128)(2,1)S(1)}, bf16[256,256]{1,0:T(8,128)(2,1)}, u32[]{:S(2)}, u32[]{:S(2)}) %collective-permute-start.1) | collective-permute-done | bytes 131104 | tf_op jit(solution)/shard_map/ppermute | solution.py:171
  24.3 7.7 %collective-permute-done.2 = bf16[256,256]{1,0:T(8,128)(2,1)} collective-permute-done((bf16[256,256]{1,0:T(8,128)(2,1)}, bf16[256,256]{1,0:T(8,128)(2,1)}, u32[]{:S(2)}, u32[]{:S(2)}) %collective-permute-start.2) | collective-permute-done | bytes 131104 | tf_op jit(solution)/shard_map/ppermute | solution.py:171
  32.1 7.9 %collective-permute-done.3 = bf16[256,256]{1,0:T(8,128)(2,1)} collective-permute-done((bf16[256,256]{1,0:T(8,128)(2,1)}, bf16[256,256]{1,0:T(8,128)(2,1)}, u32[]{:S(2)}, u32[]{:S(2)}) %collective-permute-start.3) | collective-permute-done | bytes 131104 | tf_op jit(solution)/shard_map/ppermute | solution.py:171
  40.0 11.3 %while.39 = (s32[]{:T(128)}, f32[2,128,128]{2,1,0:T(8,128)S(1)}, f32[2,128]{1,0:T(2,128)S(1)}, f32[2]{0:T(128)S(1)}, f32[2,2,256,128]{3,2,0,1:T(8,128)S(1)}, /*i...) while((s32[]{:T(128)}, f32[2,128,128]{2,1,0:T(8,128)S(1)}, ...), condition=%wide.region_6.7_spmd.clone, body=%wide.region_0.6_spmd.clone.sunk | while | flops 607329536 | bytes 4625314 | solution.py:116
  43.8 1.1 fusion.125
  49.5 1.1 fusion.125
  54.2 6.1 %collective-permute-done.5 = bf16[256,256]{1,0:T(8,128)(2,1)S(1)} collective-permute-done((bf16[256,256]{1,0:T(8,128)(2,1)}, bf16[256,256]{1,0:T(8,128)(2,1)S(1)}, u32[]{:S(2)}, u32[]{:S(2)}) %collective-permute-start.5) | collective-permute-done | bytes 131104 | tf_op jit(solution)/shard_map/ppermute | solution.py:171
  60.5 21.9 %all-reduce.4 = (f32[16]{0:T(128)S(1)}, f32[16]{0:T(128)S(1)}) all-reduce(f32[16]{0:T(128)S(1)} %bitcast_dynamic-update-slice_fusion.1, f32[16]{0:T(128)S(1)} %dynamic-update-slice.1), channel_id=2, replica_groups=mesh['sp'=8,'tp'=4] {'sp'}, use_global_device_ids=true, to_apply=%add.1 | all-reduce | flops 32 | bytes 256
  82.6 16.4 %all-gather.4 = f32[8,2,128]{2,1,0:T(2,128)S(1)} all-gather(f32[1,2,128]{2,1,0:T(2,128)S(1)} %bitcast.293), channel_id=5, replica_groups=mesh['sp'=8,'tp'=4] {'sp'}, dimensions={0}, use_global_device_ids=true | all-gather | bytes 9216 | tf_op jit(solution)/shard_map/all_gather | solution.py:13
  99.0 0.9 constant_dynamic-update-slice_fusion.13
  99.9 0.9 constant_dynamic-update-slice_fusion.12
  100.9 0.9 constant_dynamic-update-slice_fusion.11
  101.8 0.9 constant_dynamic-update-slice_fusion.10
  102.8 0.9 constant_dynamic-update-slice_fusion.5
  103.7 0.9 constant_dynamic-update-slice_fusion.4
  104.6 0.9 constant_dynamic-update-slice_fusion.3
  105.5 0.9 constant_dynamic-update-slice_fusion.2
  106.6 9.0 %while.40 = (s32[]{:T(128)}, f32[2,128,128]{2,1,0:T(8,128)S(1)}, f32[2,128]{1,0:T(2,128)S(1)}, f32[2]{0:T(128)S(1)}, s32[]{:T(128)}, /*index=5*/f32[8,2]{1,0:T(8...) while((s32[]{:T(128)}, f32[2,128,128]{2,1,0:T(8,128)S(1)}, ...), condition=%wide.region_10.11_spmd.clone, body=%wide.region_9.10_spmd.clone.sunk | while | flops 165138 | bytes 396541 | solution.py:23
  106.7 1.0 fusion.126
  107.8 1.0 fusion.126
  108.9 1.0 fusion.126
  110.1 1.0 fusion.126
  111.2 1.0 fusion.126
  112.3 1.0 fusion.126
  113.4 1.0 fusion.126
  114.5 1.0 fusion.126
  116.3 1.2 fusion.47
  117.5 2.1 bitcast_convert_fusion
  122.0 1.6 scatter_custom_fusion
  123.7 25.9 %reduce-scatter.3.cloned.1.call-done = bf16[128,2048]{1,0:T(8,128)(2,1)} async-done(((bf16[512,2048]{1,0:T(8,128)(2,1)}), bf16[128,2048]{1,0:T(8,128)(2,1)}) %reduce-scatter.3.cloned.1.call-update) | async-done | bytes 524304 | tf_op jit(solution)/shard_map/reduce_scatter | solution.py:179
  149.6 1.3 fusion.48
  150.9 1.2 fusion.50
  152.2 2.4 gather_fusion
  154.7 36.6 %all_to_all.10 = bf16[8,1,40,2048]{3,2,1,0:T(8,128)(2,1)} all-to-all(bf16[8,1,40,2048]{3,2,1,0:T(8,128)(2,1)S(1)} %bitcast.275), channel_id=1, replica_groups=mesh['sp'=8,'tp'=4] {'sp'}, dimensions={0} | all-to-all | bytes 2621440 | tf_op jit(solution)/shard_map/all_to_all | solution.py:201
  191.4 38.6 %all-gather.8.cloned.1.call-done = bf16[8,4,40,2048]{3,2,1,0:T(8,128)(2,1)} async-done(((bf16[8,1,40,2048]{3,2,1,0:T(8,128)(2,1)}), bf16[8,4,40,2048]{3,2,1,0:T(8,128)(2,1)}) %all-gather.8.cloned.1.call-update) | async-done | bytes 5242896 | tf_op jit(solution)/shard_map/all_gather | solution.py:200
  230.0 10.0 %fusion.43 = f32[1280,896]{1,0:T(8,128)} fusion(bf16[1280,2048]{1,0:T(8,128)(2,1)} %bitcast.302, bf16[1,2048,896]{2,1,0:T(8,128)(2,1)} %param.27), kind=kOutput, calls=%fused_computation.81 | convolution fusion | flops 4697620480 | bytes 13500416 | tf_op jit(solution)/shard_map/dot_general | solution.py:214
  240.0 17.6 %convolution_convert_fusion = bf16[1280,2048]{1,0:T(8,128)(2,1)} fusion(bf16[1,896,2048]{2,1,0:T(8,128)(2,1)} %param.29, f32[1280,896]{1,0:T(8,128)} %fusion.43, bf16[1280,2048]{1,0:T(8,128)(2,1)} %bitcast.303, bf16[1,2048,896]{2,1,0:T(8,128)(2,1)} %param.28), kind=kOutput, calls=%fused_computation.76 | convolution fusion | flops 9404743680 | bytes 22413312 | tf_op jit(solution)/shard_map/dot_general | solution.py:217
  258.8 101.5 %all-reduce.7.cloned.1.call-done = bf16[8,4,40,2048]{3,2,1,0:T(8,128)(2,1)} async-done(((bf16[8,4,40,2048]{3,2,1,0:T(8,128)(2,1)}), bf16[8,4,40,2048]{3,2,1,0:T(8,128)(2,1)}) %all-reduce.7.cloned.1.call-update) | async-done | bytes 5242896
  360.2 3.2 constant_dynamic-slice_fusion.3
  363.5 5.5 %all-to-all-start.1 = ((bf16[8,1,40,2048]{3,2,1,0:T(8,128)(2,1)}), bf16[8,1,40,2048]{3,2,1,0:T(8,128)(2,1)S(1)}, u32[]{:S(2)}, u32[]{:S(2)}) async-start(bf16[8,1,40,2048]{3,2,1,0:T(8,128)(2,1)} %constant_dynamic-slice_fusion.3), calls=%async_computation.2 | async-start | bytes 2621440 | tf_op jit(solution)/shard_map/all_to_all | solution.py:225
  369.1 30.9 %all-to-all-done.1 = bf16[8,1,40,2048]{3,2,1,0:T(8,128)(2,1)S(1)} async-done(((bf16[8,1,40,2048]{3,2,1,0:T(8,128)(2,1)}), bf16[8,1,40,2048]{3,2,1,0:T(8,128)(2,1)S(1)}, u32[]{:S(2)}, u32[]{:S(2)}) %all-to-all-start.1) | async-done | bytes 1310752 | tf_op jit(solution)/shard_map/all_to_all | solution.py:225
  400.0 2.3 gather_fusion.1
  402.4 2.4 reshape.428
  404.7 3.2 multiply_reduce_fusion
  407.9 1.0 fusion.51
  (185 shorter events, 18.4 us)
Async XLA Ops:
  6.5 4.4 %copy-start.4 = (bf16[512,256]{1,0:T(8,128)(2,1)S(1)}, bf16[512,256]{1,0:T(8,128)(2,1)}, u32[]{:S(2)}) copy-start(bf16[512,256]{1,0:T(8,128)(2,1)} %param.19) | copy-start | bytes 786436
  6.5 100.1 %all-gather.10.cloned.1.call-start = ((), (), s32[]{:S(2)}) async-start(), calls=%async_computation.5 | async-start | bytes 1179648 | tf_op jit(solution)/shard_map/all_gather | solution.py:13
  6.5 9.7 %collective-permute-start = (bf16[256,256]{1,0:T(8,128)(2,1)}, bf16[256,256]{1,0:T(8,128)(2,1)S(1)}, u32[]{:S(2)}, u32[]{:S(2)}) collective-permute-start(bf16[256,256]{1,0:T(8,128)(2,1)} %param.25), channel_id=1, source_target_pairs={{0,4},{4,8},{8,12},{12,16},{16,20},{20,24},{24,28},{28,0},{1,5},{5... | collective-permute-start | bytes 393224 | tf_op jit(solution)/shard_map/ppermute | solution.py:171
  10.6 5.9 %copy-start.5 = (bf16[512,256]{1,0:T(8,128)(2,1)S(1)}, bf16[512,256]{1,0:T(8,128)(2,1)}, u32[]{:S(2)}) copy-start(bf16[512,256]{1,0:T(8,128)(2,1)} %param.20) | copy-start | bytes 786436
  16.3 7.8 %collective-permute-start.1 = (bf16[256,256]{1,0:T(8,128)(2,1)S(1)}, bf16[256,256]{1,0:T(8,128)(2,1)}, u32[]{:S(2)}, u32[]{:S(2)}) collective-permute-start(bf16[256,256]{1,0:T(8,128)(2,1)S(1)} %collective-permute-done), channel_id=1, source_target_pairs={{0,4},{4,8},{8,12},{12,16},{16,20},{20,24},{24,28},{28,0},{1,5},{5... | collective-permute-start | bytes 393224 | tf_op jit(solution)/shard_map/ppermute | solution.py:171
  16.3 15.8 %copy-start.8 = (f32[2,512]{1,0:T(2,128)S(1)}, f32[2,512]{1,0:T(2,128)}, u32[]{:S(2)}) copy-start(f32[2,512]{1,0:T(2,128)} %param.23) | copy-start | bytes 12292
  16.3 15.8 %copy-start.9 = (f32[2,512]{1,0:T(2,128)S(1)}, f32[2,512]{1,0:T(2,128)}, u32[]{:S(2)}) copy-start(f32[2,512]{1,0:T(2,128)} %param.22) | copy-start | bytes 12292
  16.3 23.7 %copy-start.6 = (f32[2,512]{1,0:T(2,128)S(1)}, f32[2,512]{1,0:T(2,128)}, u32[]{:S(2)}) copy-start(f32[2,512]{1,0:T(2,128)} %param.21) | copy-start | bytes 12292
  24.0 8.0 %collective-permute-start.2 = (bf16[256,256]{1,0:T(8,128)(2,1)}, bf16[256,256]{1,0:T(8,128)(2,1)}, u32[]{:S(2)}, u32[]{:S(2)}) collective-permute-start(bf16[256,256]{1,0:T(8,128)(2,1)} %collective-permute-done.1), channel_id=1, source_target_pairs={{0,4},{4,8},{8,12},{12,16},{16,20},{20,24},{24,28},{28,0},{1,5},{5... | collective-permute-start | bytes 393224 | tf_op jit(solution)/shard_map/ppermute | solution.py:171
  32.0 8.0 %collective-permute-start.3 = (bf16[256,256]{1,0:T(8,128)(2,1)}, bf16[256,256]{1,0:T(8,128)(2,1)}, u32[]{:S(2)}, u32[]{:S(2)}) collective-permute-start(bf16[256,256]{1,0:T(8,128)(2,1)} %collective-permute-done.2), channel_id=1, source_target_pairs={{0,4},{4,8},{8,12},{12,16},{16,20},{20,24},{24,28},{28,0},{1,5},{5... | collective-permute-start | bytes 393224 | tf_op jit(solution)/shard_map/ppermute | solution.py:171
  40.0 12.4 %collective-permute-start.4 = (bf16[256,256]{1,0:T(8,128)(2,1)}, bf16[256,256]{1,0:T(8,128)(2,1)}, u32[]{:S(2)}, u32[]{:S(2)}) collective-permute-start(bf16[256,256]{1,0:T(8,128)(2,1)} %collective-permute-done.3), channel_id=1, source_target_pairs={{0,4},{4,8},{8,12},{12,16},{16,20},{20,24},{24,28},{28,0},{1,5},{5... | collective-permute-start | bytes 393224 | tf_op jit(solution)/shard_map/ppermute | solution.py:171
  40.0 12.6 %copy-start.12 = (u32[32]{0:T(128)S(1)}, u32[32]{0:T(128)}, u32[]{:S(2)}) copy-start(u32[32]{0:T(128)} %constant.149) | copy-start | bytes 388
  51.4 9.1 %copy-start = (f32[2,128,128]{2,1,0:T(8,128)}, f32[2,128,128]{2,1,0:T(8,128)S(1)}, u32[]{:S(2)}) copy-start(f32[2,128,128]{2,1,0:T(8,128)S(1)} %get-tuple-element.230) | copy-start | bytes 393220
  51.4 51.3 %copy-start.3 = (bf16[256,256]{1,0:T(8,128)(2,1)S(1)}, bf16[256,256]{1,0:T(8,128)(2,1)}, u32[]{:S(2)}) copy-start(bf16[256,256]{1,0:T(8,128)(2,1)} %param.25) | copy-start | bytes 393220
  52.4 8.0 %collective-permute-start.5 = (bf16[256,256]{1,0:T(8,128)(2,1)}, bf16[256,256]{1,0:T(8,128)(2,1)S(1)}, u32[]{:S(2)}, u32[]{:S(2)}) collective-permute-start(bf16[256,256]{1,0:T(8,128)(2,1)} %collective-permute-done.4), channel_id=1, source_target_pairs={{0,4},{4,8},{8,12},{12,16},{16,20},{20,24},{24,28},{28,0},{1,5},{5... | collective-permute-start | bytes 393224 | tf_op jit(solution)/shard_map/ppermute | solution.py:171
  60.3 38.6 %collective-permute-start.6 = (bf16[256,256]{1,0:T(8,128)(2,1)S(1)}, bf16[256,256]{1,0:T(8,128)(2,1)S(1)}, u32[]{:S(2)}, u32[]{:S(2)}) collective-permute-start(bf16[256,256]{1,0:T(8,128)(2,1)S(1)} %collective-permute-done.5), channel_id=1, source_target_pairs={{0,4},{4,8},{8,12},{12,16},{16,20},{20,24},{24,28},{28,0},{1,5},{5... | collective-permute-start | bytes 393224 | tf_op jit(solution)/shard_map/ppermute | solution.py:171
  60.5 89.2 %reduce-scatter.3.cloned.1.call-start = ((), (), s32[]{:S(2)}) async-start(), calls=%async_computation.3 | async-start | bytes 2621440 | tf_op jit(solution)/shard_map/reduce_scatter | solution.py:179
  119.6 30.1 %copy-start.1 = (bf16[128,2048]{1,0:T(8,128)(2,1)S(1)}, bf16[128,2048]{1,0:T(8,128)(2,1)}, u32[]{:S(2)}) copy-start(bf16[128,2048]{1,0:T(8,128)(2,1)} %param.24) | copy-start | bytes 1572868
  119.6 31.4 %copy-start.7 = (f32[2048]{0:T(1024)S(1)}, f32[2048]{0:T(1024)}, u32[]{:S(2)}) copy-start(f32[2048]{0:T(1024)} %param.26) | copy-start | bytes 24580
  119.6 110.4 %all-gather.8.cloned.1.call-start = ((), (), s32[]{:S(2)}) async-start(), calls=%async_computation.4 | async-start | bytes 6553600 | tf_op jit(solution)/shard_map/all_gather | solution.py:200
  191.3 168.9 %all-reduce.7.cloned.1.call-start = ((), (), s32[]{:S(2)}) async-start(), calls=%async_computation.6 | async-start | bytes 10485760
  257.5 0.7 copy-start.11
  360.2 8.7 %copy-start.10 = (f32[128,2]{0,1:T(2,128)S(1)}, f32[128,2]{0,1:T(2,128)}, u32[]{:S(2)}) copy-start(f32[128,2]{0,1:T(2,128)} %param.31) | copy-start | bytes 3076
  363.5 36.5 %all-to-all-start.1 = ((bf16[8,1,40,2048]{3,2,1,0:T(8,128)(2,1)}), bf16[8,1,40,2048]{3,2,1,0:T(8,128)(2,1)S(1)}, u32[]{:S(2)}, u32[]{:S(2)}) async-start(bf16[8,1,40,2048]{3,2,1,0:T(8,128)(2,1)} %constant_dynamic-slice_fusion.3), calls=%async_computation.2 | async-start | bytes 2621440 | tf_op jit(solution)/shard_map/all_to_all | solution.py:225
  404.7 3.2 copy-start.2
Sparse Core Ops, SparseCore 0:
  60.6 41.8 all-gather.9
  119.7 29.8 reduce-scatter.2
  191.5 38.4 all-gather.7
  257.7 102.5 all-reduce.6
